TPU v7x, 32 devices: a whole 2x2x4 slice. The times are simulated.
32 devices in a mesh: fs: 4 (over z), rep: 4 (over y, x), tp: 2 (over core).
Axes of the slice: x: 2, y: 2, z: 4, core: 2. Of those that a mesh axis runs over, the one named last changes fastest.
Arguments:
- mixer_input: bfloat16 [32768, 2048], P(('fs', 'rep')), may hold values from -6 to 6
- value_cot: bfloat16 [32768, 2048], P(('fs', 'rep'), 'tp'), may hold values from -0.22097087 to 0.22097087
- gate_cot: bfloat16 [32768, 2048], P(('fs', 'rep'), 'tp'), may hold values from -0.22097087 to 0.22097087
- value_weight: float32 [2048, 2048], P('fs', 'tp'), may hold values from -0.125 to 0.125
- gate_weight: float32 [2048, 2048], P('fs', 'tp'), may hold values from -0.125 to 0.125
- value_basis: bfloat16 [2048, 256], replicated, may hold values from -0.8838835 to 0.8838835
- gate_basis: bfloat16 [2048, 256], replicated, may hold values from -0.8838835 to 0.8838835
- value_first: float32 [256, 2048], P('fs', 'tp'), may hold values from -6 to 6
- gate_first: float32 [256, 2048], P('fs', 'tp'), may hold values from -6 to 6
- value_second: float32 [256, 2048], P('fs', 'tp'), may hold values from 0.01 to 1
- gate_second: float32 [256, 2048], P('fs', 'tp'), may hold values from 0.01 to 1
Outputs:
- value_new: float32 [2048, 2048], P('fs', 'tp')
- gate_new: float32 [2048, 2048], P('fs', 'tp')
- value_copy: bfloat16 [2048, 2048], P(None, 'tp')
- gate_copy: bfloat16 [2048, 2048], P(None, 'tp')
- value_step: float32 [2048, 2048], P('fs', 'tp')
- gate_step: float32 [2048, 2048], P('fs', 'tp')
- value_first_new: float32 [256, 2048], P('fs', 'tp')
- gate_first_new: float32 [256, 2048], P('fs', 'tp')
- value_second_new: float32 [256, 2048], P('fs', 'tp')
- gate_second_new: float32 [256, 2048], P('fs', 'tp')
All inputs are finite; a program needn't handle non-finite values.
Results may differ from a plain program's by a relative error of at most 0.0044.
Values may be sent and summed in bfloat16 or wider, within the bound.
A program may use at most 128 MiB of HBM per device.

v0:
```python
import functools

import jax
import jax.numpy as jnp
from jax import lax
from jax.experimental import pallas as pl
from jax.experimental.pallas import tpu as pltpu
from jax.sharding import PartitionSpec as P

learn_rate = 0.02
CHUNKS = 4
F32 = jnp.float32
BF16 = jnp.bfloat16


def dot(a, b):
    return jnp.dot(a, b, preferred_element_type=F32)


def dot_first(a, b):
    return lax.dot_general(a, b, (((0,), (0,)), ((), ())), preferred_element_type=F32)


def split(a):
    upper = a.astype(BF16)
    return upper, (a - upper.astype(F32)).astype(BF16)


def exchange(
    n_fs, n_rep, n_tp,
    mixer, value_cot, gate_cot, value_weight, gate_weight, value_basis, gate_basis,
    value_first_hbm, gate_first_hbm, value_second_hbm, gate_second_hbm,
    value_rows, gate_rows, scaled_out, projected_out, squares_out,
    x_buf, cot_buf, w_buf, w_half, basis_buf, gram, acc, part_in,
    mid, mid_in, proj_all, scaled, sq_buf, moments,
    x_sem, w_sem, b_sem, own_sem, m_sem,
    w1_send, w1_recv, w2_send, w2_recv,
    s1_send, s1_recv, s2_send, s2_recv, p_send, p_recv, a_send, a_recv, g_send, g_recv, q_send, q_recv,
):
    f, r, t = lax.axis_index("fs"), lax.axis_index("rep"), lax.axis_index("tp")
    cots = (value_cot, gate_cot)
    weights = (value_weight, gate_weight)
    bases = (value_basis, gate_basis)
    gathered = (value_rows, gate_rows)
    tokens = mixer.shape[0]
    chunk = tokens // CHUNKS
    rows = value_weight.shape[0]
    share = rows // n_rep
    width = acc.shape[2]
    per_role = n_rep // 2
    low = mid.shape[1]

    def fs_at(d):
        return lax.rem(f + d, n_fs)

    def rep_at(d):
        return lax.rem(r + d, n_rep)

    def send(src, dst, s, v, **where):
        return pltpu.make_async_remote_copy(
            src_ref=src, dst_ref=dst, send_sem=s, recv_sem=v,
            device_id=where, device_id_type=pl.DeviceIdType.MESH,
        )

    w_loads = [pltpu.make_async_copy(weights[k], w_buf.at[k], w_sem.at[k]) for k in range(2)]
    b_loads = [pltpu.make_async_copy(bases[k], basis_buf.at[k], b_sem.at[k]) for k in range(2)]

    def x_loads(c):
        span = pl.ds(pl.multiple_of(c * chunk, chunk), chunk)
        return [pltpu.make_async_copy(mixer.at[span], x_buf.at[c], x_sem.at[c, 0])] + [
            pltpu.make_async_copy(cots[k].at[span], cot_buf.at[k, c], x_sem.at[c, 1 + k]) for k in range(2)
        ]

    m_loads = [
        pltpu.make_async_copy(ref, moments.at[i], m_sem.at[i])
        for i, ref in enumerate((value_first_hbm, gate_first_hbm, value_second_hbm, gate_second_hbm))
    ]
    for copy in w_loads + b_loads:
        copy.start()
    for c in range(CHUNKS):
        for copy in x_loads(c):
            copy.start()

    for copy in m_loads:
        copy.start()

    barrier = pltpu.get_barrier_semaphore()
    for d in range(1, n_fs):
        pl.semaphore_signal(barrier, inc=1, device_id={"fs": fs_at(d)}, device_id_type=pl.DeviceIdType.MESH)
    for d in range(1, n_rep):
        pl.semaphore_signal(barrier, inc=1, device_id={"rep": rep_at(d)}, device_id_type=pl.DeviceIdType.MESH)
    for d in range(1, n_tp):
        pl.semaphore_signal(
            barrier, inc=1, device_id={"tp": lax.rem(t + d, n_tp)}, device_id_type=pl.DeviceIdType.MESH
        )
    for k in range(2):
        w_loads[k].wait()
        w_half[k] = w_buf[k].astype(BF16)
    pl.semaphore_wait(barrier, n_fs + n_rep + n_tp - 3)

    def share_of(block, part_index):
        return pl.ds(pl.multiple_of(block * rows + part_index * share, share), share)

    w1 = {}
    for d in range(1, n_fs):
        for k in range(2):
            w1[d, k] = send(
                w_half.at[k, pl.ds(pl.multiple_of(r * share, share), share)],
                gathered[k].at[share_of(f, r)],
                w1_send.at[d - 1, k], w1_recv.at[d - 1, k], fs=fs_at(d),
            )
            w1[d, k].start()
    own = []
    for k in range(2):
        copy = pltpu.make_async_copy(
            w_half.at[k], gathered[k].at[pl.ds(pl.multiple_of(f * rows, rows), rows)], own_sem.at[k]
        )
        copy.start()
        own.append(copy)

    for copy in b_loads:
        copy.wait()
    acc[...] = jnp.zeros_like(acc)

    def one_chunk(c, carry):
        for copy in x_loads(c):
            copy.wait()
        x = x_buf[c]
        for k in range(2):
            upper, lower = split(dot(x, basis_buf[k]))
            for q in range(per_role):
                cols = slice(q * width, (q + 1) * width)
                cot = cot_buf[k, c, :, cols]
                acc[k * per_role + q] += dot_first(upper, cot) + dot_first(lower, cot)
        return carry

    lax.fori_loop(0, CHUNKS, one_chunk, 0)
    s1 = {}
    for d in range(1, n_rep):
        s1[d] = send(
            acc.at[rep_at(d)], part_in.at[d - 1], s1_send.at[d - 1], s1_recv.at[d - 1], rep=rep_at(d)
        )
        s1[d].start()

    w2, heard = {}, set()
    near, far = (r + 1 - 2 * lax.rem(r, 2), lax.rem(r + 2, n_rep)) if n_rep == 4 else (None, None)

    def pass_on(d, e, k, owner, peer):
        source = lax.rem(f - d + n_fs, n_fs)
        rows_ref = gathered[k].at[share_of(source, owner)]
        w2[d, e, k] = send(
            rows_ref, rows_ref, w2_send.at[d - 1, e, k], w2_recv.at[d - 1, e, k], rep=peer
        )
        w2[d, e, k].start()

    def forward(d):
        for k in range(2):
            w1[d, k].wait_recv()
            peers = (near, far) if n_rep == 4 else [rep_at(e) for e in range(1, n_rep)]
            for e, peer in enumerate(peers):
                pass_on(d, e, k, r, peer)

    def relay(d):
        if n_rep == 4:
            for e, k, owner, peer in ((0, 0, near, far), (1, 1, far, near)):
                w2[d, e, k].wait_recv()
                heard.add((d, e, k))
                pass_on(d, 2, k, owner, peer)

    forward(1)
    for k in range(2):
        upper, lower = split(dot_first(basis_buf[k], basis_buf[k]))
        gram[k, 0] = upper
        gram[k, 1] = lower

    for d in range(1, n_rep):
        s1[d].wait_recv()
    total = acc[r]
    for d in range(1, n_rep):
        total += part_in[d - 1]
    mid[...] = total.reshape(mid.shape)
    s2 = {}
    for d in range(1, n_fs):
        s2[d] = send(
            mid.at[fs_at(d)], mid_in.at[d - 1], s2_send.at[d - 1], s2_recv.at[d - 1], fs=fs_at(d)
        )
        s2[d].start()
    for d in range(2, n_fs - 1):
        forward(d)
        relay(d - 1)
    for d in range(1, n_fs):
        s2[d].wait_recv()
    small = mid[f]
    for d in range(1, n_fs):
        small += mid_in[d - 1]
    proj_all[r] = small.astype(BF16)

    cols = pl.ds(pl.multiple_of(lax.rem(r, per_role) * width, width), width)
    is_value = r < per_role
    for copy in m_loads:
        copy.wait()
    first = jnp.where(is_value, moments[0, :, cols], moments[1, :, cols])
    second = jnp.where(is_value, moments[2, :, cols], moments[3, :, cols])
    first_new = 0.9 * first + 0.1 * small
    second_new = 0.95 * second + 0.05 * small * small
    scaled[r, f] = (first_new * lax.rsqrt(second_new)).astype(BF16)
    a4, p4, g4 = {}, {}, {}
    for d in range(1, n_fs):
        a4[d] = send(
            scaled.at[r, f], scaled.at[r, f], a_send.at[d - 1], a_recv.at[d - 1], fs=fs_at(d)
        )
        a4[d].start()
    for d in range(1, n_rep):
        p4[d] = send(proj_all.at[r], proj_all.at[r], p_send.at[d - 1], p_recv.at[d - 1], rep=rep_at(d))
        p4[d].start()
    if n_fs > 2:
        forward(n_fs - 1)
        relay(n_fs - 2)
    for d in range(1, n_fs):
        a4[d].wait_recv()
    for d in range(1, n_rep):
        g4[d] = send(scaled.at[r], scaled.at[r], g_send.at[d - 1], g_recv.at[d - 1], rep=rep_at(d))
        g4[d].start()
    relay(n_fs - 1)
    for d in range(1, n_rep):
        g4[d].wait_recv()

    for k in range(2):
        squares = 0.0
        for q in range(per_role):
            s = scaled[k * per_role + q].reshape(n_fs * low, width)
            squares += jnp.sum((dot(gram[k, 0], s) + dot(gram[k, 1], s)) * s.astype(F32))
        sq_buf[0, k] = jnp.full(sq_buf.shape[2:], squares, F32)
    q4 = []
    for d in range(1, n_tp):
        copy = send(
            sq_buf.at[0], sq_buf.at[d], q_send.at[d - 1], q_recv.at[d - 1], tp=lax.rem(t + d, n_tp)
        )
        copy.start()
        q4.append(copy)
    for d in range(1, n_rep):
        p4[d].wait_recv()
    scaled_out[...] = scaled[...].reshape(scaled_out.shape)
    projected_out[...] = proj_all[...]
    for copy in q4:
        copy.wait_recv()
    sums = sq_buf[0]
    for d in range(1, n_tp):
        sums += sq_buf[d]
    squares_out[...] = sums

    for copy in list(w1.values()) + list(s1.values()) + list(s2.values()) + list(a4.values()):
        copy.wait_send()
    for copy in list(p4.values()) + list(g4.values()) + q4:
        copy.wait_send()
    for copy in own:
        copy.wait()
    for key, copy in w2.items():
        copy.wait_send()
        if key not in heard:
            copy.wait_recv()


def finish(
    own_blocks, entries,
    where, value_rows, gate_rows, value_basis, gate_basis, value_weight, gate_weight,
    scaled, projected, squares, value_first, gate_first, value_second, gate_second,
    value_new, gate_new, value_copy, gate_copy, value_step, gate_step,
    value_first_new, gate_first_new, value_second_new, gate_second_new,
):
    step = pl.program_id(0)
    width = scaled.shape[2]
    per_role = scaled.shape[0] // 2
    roles = (
        (value_rows, value_basis, value_weight, value_new, value_copy, value_step),
        (gate_rows, gate_basis, gate_weight, gate_new, gate_copy, gate_step),
    )
    for k, (rows, basis, weight, new, copy, step_out) in enumerate(roles):
        factor = lax.rsqrt(squares[k, :1, :1] / entries + 1e-06)
        for q in range(per_role):
            cols = slice(q * width, (q + 1) * width)
            direction = dot(basis[...], scaled[k * per_role + q]) * factor
            copy[:, cols] = (rows[:, cols].astype(F32) - learn_rate * direction).astype(BF16)

            @pl.when(step < own_blocks)
            def _():
                step_out[:, cols] = direction
                new[:, cols] = weight[:, cols] - learn_rate * direction

    @pl.when(step == 0)
    def _():
        moments = (
            (value_first, value_second, value_first_new, value_second_new),
            (gate_first, gate_second, gate_first_new, gate_second_new),
        )
        for k, (first, second, first_new, second_new) in enumerate(moments):
            for q in range(per_role):
                cols = slice(q * width, (q + 1) * width)
                small = projected[k * per_role + q].astype(F32)
                first_new[:, cols] = 0.9 * first[:, cols] + 0.1 * small
                second_new[:, cols] = 0.95 * second[:, cols] + 0.05 * small * small


def local(sizes, *args):
    n_fs, n_rep, n_tp = sizes
    (mixer, value_cot, gate_cot, value_weight, gate_weight, value_basis, gate_basis,
     value_first, gate_first, value_second, gate_second) = args
    tokens, model = mixer.shape
    half = value_cot.shape[1]
    rows = value_weight.shape[0]
    rank = value_basis.shape[1]
    low = value_first.shape[0]
    width = 2 * half // n_rep
    chunk = tokens // CHUNKS
    any_spec = pl.BlockSpec(memory_space=pl.ANY)
    vmem = pl.BlockSpec(memory_space=pltpu.VMEM)
    dma = pltpu.SemaphoreType.DMA
    scratch = [
        pltpu.VMEM((CHUNKS, chunk, model), BF16),
        pltpu.VMEM((2, CHUNKS, chunk, half), BF16),
        pltpu.VMEM((2, rows, half), F32),
        pltpu.VMEM((2, rows, half), BF16),
        pltpu.VMEM((2, model, rank), BF16),
        pltpu.VMEM((2, 2, rank, rank), BF16),
        pltpu.VMEM((n_rep, rank, width), F32),
        pltpu.VMEM((n_rep - 1, rank, width), F32),
        pltpu.VMEM((n_fs, low, width), F32),
        pltpu.VMEM((n_fs - 1, low, width), F32),
        pltpu.VMEM((n_rep, low, width), BF16),
        pltpu.VMEM((n_rep, n_fs, low, width), BF16),
        pltpu.VMEM((n_tp, 2, 8, 128), F32),
        pltpu.VMEM((4, low, half), F32),
        dma((CHUNKS, 3)), dma((2,)), dma((2,)), dma((2,)), dma((4,)),
        dma((n_fs - 1, 2)), dma((n_fs - 1, 2)),
        dma((n_fs - 1, n_rep - 1, 2)), dma((n_fs - 1, n_rep - 1, 2)),
    ]
    for count in (n_rep, n_fs, n_rep, n_fs, n_rep, n_tp):
        scratch += [dma((count - 1,)), dma((count - 1,))]
    value_rows, gate_rows, scaled, projected, squares = pl.pallas_call(
        functools.partial(exchange, n_fs, n_rep, n_tp),
        out_shape=(
            jax.ShapeDtypeStruct((rows * n_fs, half), BF16),
            jax.ShapeDtypeStruct((rows * n_fs, half), BF16),
            jax.ShapeDtypeStruct((n_rep, rank, width), BF16),
            jax.ShapeDtypeStruct((n_rep, low, width), BF16),
            jax.ShapeDtypeStruct((2, 8, 128), F32),
        ),
        in_specs=[any_spec] * 11,
        out_specs=(any_spec, any_spec, vmem, vmem, vmem),
        scratch_shapes=scratch,
        compiler_params=pltpu.CompilerParams(
            collective_id=0, has_side_effects=True, vmem_limit_bytes=52 * 1024 * 1024
        ),
        name="exchange",
    )(*args)

    block = min(rows, 256)
    own_blocks = rows // block
    blocks = model // block
    where = (lax.axis_index("fs") * own_blocks).astype(jnp.int32).reshape(1)

    def turned(i, w):
        return (lax.rem(w[0] + i, blocks), 0)

    def own(i, w):
        return (jnp.minimum(i, own_blocks - 1), 0)

    def whole(shape):
        return pl.BlockSpec(shape, lambda i, w: (0,) * len(shape))

    row_spec = pl.BlockSpec((block, half), turned)
    basis_spec = pl.BlockSpec((block, rank), turned)
    own_spec = pl.BlockSpec((block, half), own)
    moment = whole((low, half))
    return pl.pallas_call(
        functools.partial(finish, own_blocks, float(model) * half * n_tp),
        grid_spec=pltpu.PrefetchScalarGridSpec(
            num_scalar_prefetch=1,
            grid=(blocks,),
            in_specs=[row_spec, row_spec, basis_spec, basis_spec, own_spec, own_spec,
                      whole(scaled.shape), whole(projected.shape), whole(squares.shape)] + [moment] * 4,
            out_specs=[own_spec, own_spec, row_spec, row_spec, own_spec, own_spec] + [moment] * 4,
        ),
        out_shape=[
            jax.ShapeDtypeStruct((rows, half), F32),
            jax.ShapeDtypeStruct((rows, half), F32),
            jax.ShapeDtypeStruct((model, half), BF16),
            jax.ShapeDtypeStruct((model, half), BF16),
            jax.ShapeDtypeStruct((rows, half), F32),
            jax.ShapeDtypeStruct((rows, half), F32),
        ] + [jax.ShapeDtypeStruct((low, half), F32)] * 4,
        compiler_params=pltpu.CompilerParams(vmem_limit_bytes=40 * 1024 * 1024),
        name="finish",
    )(where, value_rows, gate_rows, value_basis, gate_basis, value_weight, gate_weight,
      scaled, projected, squares, value_first, gate_first, value_second, gate_second)


def solution(mesh):
    sizes = tuple(mesh.shape[name] for name in ("fs", "rep", "tp"))
    return jax.shard_map(
        lambda *args: tuple(local(sizes, *args)),
        mesh=mesh,
        in_specs=(
            P(("fs", "rep"), None),
            P(("fs", "rep"), "tp"),
            P(("fs", "rep"), "tp"),
            P("fs", "tp"),
            P("fs", "tp"),
            P(),
            P(),
            P("fs", "tp"),
            P("fs", "tp"),
            P("fs", "tp"),
            P("fs", "tp"),
        ),
        out_specs=(
            P("fs", "tp"),
            P("fs", "tp"),
            P(None, "tp"),
            P(None, "tp"),
            P("fs", "tp"),
            P("fs", "tp"),
            P("fs", "tp"),
            P("fs", "tp"),
            P("fs", "tp"),
            P("fs", "tp"),
        ),
        check_vma=False,
    )
```

profile of v0, /device:TPU:0, one launch (start us, length us, event | category | flops | bytes accessed | tf_op | source)
XLA Modules:
  0.0 137.1 jit_solution(11721257788102966021)
XLA Ops:
  0.7 0.0 copy-start.5
  0.7 0.9 copy-done.5
  1.6 0.0 copy-start.7
  1.6 0.9 copy-done.7
  2.6 0.0 copy-start.9
  2.6 0.9 copy-done.9
  3.5 0.0 copy-start.10
  3.5 0.9 copy-done.10
  4.5 0.0 copy-start
  4.5 0.0 copy-start.1
  4.5 0.0 copy-start.3
  4.5 0.0 copy-start.4
  4.5 0.0 copy-start.6
  4.5 0.0 copy-start.8
  4.5 114.6 %exchange.1 = (bf16[2048,1024]{1,0:T(8,128)(2,1)}, bf16[2048,1024]{1,0:T(8,128)(2,1)}, bf16[4,256,512]{2,1,0:T(8,128)(2,1)}, bf16[4,64,512]{2,1,0:T(8,128)(2,1)S(1)}, f32[2,8,128]{2,1,0:T(8,128)S(1)}) custom-call(bf16[2048,2048]{1,0:T(8,128)(2,1)} %mixer.1, bf16[2048,1024]{1,0:T(8,128)(2,1)} %value_cot.1, bf16[2048,1024]{1,0:T(8,128)(2,1)} %gate_cot.1, ...), custom_call_target="tpu_custom_call" | custom-call | tf_op jit(solution)/shard_map/exchange/pallas_call | solution.py:339
  119.1 0.0 copy-done
  119.1 0.0 copy-done.1
  119.1 0.0 copy-done.3
  119.1 0.0 copy-done.4
  119.2 0.0 copy-done.6
  119.2 0.0 copy-done.8
  119.2 0.0 copy-start.2
  119.2 2.2 %copy-done.2 = bf16[2048,1024]{1,0:T(8,128)(2,1)S(1)} copy-done((bf16[2048,1024]{1,0:T(8,128)(2,1)S(1)}, bf16[2048,1024]{1,0:T(8,128)(2,1)}, u32[]{:S(2)}) %copy-start.2) | copy-done | bytes 4194328
  121.4 0.0 copy-start.11
  121.4 1.2 copy-done.11
  122.6 14.5 %finish.1 = (f32[512,1024]{1,0:T(8,128)}, f32[512,1024]{1,0:T(8,128)}, bf16[2048,1024]{1,0:T(8,128)(2,1)}, bf16[2048,1024]{1,0:T(8,128)(2,1)}, f32[512,1024]{1,0...) custom-call(s32[1]{0:T(128)} %bitcast.where, ...), custom_call_target="tpu_custom_call" | custom-call | tf_op jit(solution)/shard_map/finish/pallas_call | solution.py:375
Async XLA Ops:
  0.7 1.0 copy-start.5
  1.6 0.9 copy-start.7
  2.6 0.9 copy-start.9
  3.5 0.9 copy-start.10
  4.5 114.7 %copy-start = (f32[512,1024]{1,0:T(8,128)S(1)}, f32[512,1024]{1,0:T(8,128)}, u32[]{:S(2)}) copy-start(f32[512,1024]{1,0:T(8,128)} %value_weight.3) | copy-start | bytes 6291460
  4.5 114.7 %copy-start.1 = (f32[512,1024]{1,0:T(8,128)S(1)}, f32[512,1024]{1,0:T(8,128)}, u32[]{:S(2)}) copy-start(f32[512,1024]{1,0:T(8,128)} %gate_weight.3) | copy-start | bytes 6291460
  4.5 114.7 %copy-start.3 = (bf16[2048,256]{1,0:T(8,128)(2,1)S(1)}, bf16[2048,256]{1,0:T(8,128)(2,1)}, u32[]{:S(2)}) copy-start(bf16[2048,256]{1,0:T(8,128)(2,1)} %value_basis.3) | copy-start | bytes 3145732
  4.5 114.7 %copy-start.4 = (bf16[2048,256]{1,0:T(8,128)(2,1)S(1)}, bf16[2048,256]{1,0:T(8,128)(2,1)}, u32[]{:S(2)}) copy-start(bf16[2048,256]{1,0:T(8,128)(2,1)} %gate_basis.3) | copy-start | bytes 3145732
  4.5 114.7 %copy-start.6 = (f32[64,1024]{1,0:T(8,128)S(1)}, f32[64,1024]{1,0:T(8,128)}, u32[]{:S(2)}) copy-start(f32[64,1024]{1,0:T(8,128)} %value_first.1) | copy-start | bytes 786436
  4.5 114.7 %copy-start.8 = (f32[64,1024]{1,0:T(8,128)S(1)}, f32[64,1024]{1,0:T(8,128)}, u32[]{:S(2)}) copy-start(f32[64,1024]{1,0:T(8,128)} %gate_first.1) | copy-start | bytes 786436
  119.2 2.2 %copy-start.2 = (bf16[2048,1024]{1,0:T(8,128)(2,1)S(1)}, bf16[2048,1024]{1,0:T(8,128)(2,1)}, u32[]{:S(2)}) copy-start(bf16[2048,1024]{1,0:T(8,128)(2,1)} %get-tuple-element.15.value_rows) | copy-start | bytes 12582916
  121.4 1.2 copy-start.11
where the time goes:
time: 138 us; the launch traced here: 137 us
  Pallas kernels  129 us (93%)
  local copies, waits for them, and re-layouts  7.22 us (5%)
    pallas_call x1, Pallas kernels, local(): pl.pallas_call(functools.partial(exchange, n_fs, n_rep, n_tp), out_shape=...  115 us
    pallas_call x1, Pallas kernels, local(): pl.pallas_call(functools.partial(finish, own_blocks, float(model) * half...  14.5 us
    unnamed x24, local copies, waits for them, and re-layouts  7.22 us

commit v1 on v0

--- a/solution.py
+++ b/solution.py
@@ -9,6 +9,8 @@
 
 learn_rate = 0.02
 CHUNKS = 4
+VMEM_FIRST = 40 * 1024 * 1024
+VMEM_SECOND = 40 * 1024 * 1024
 F32 = jnp.float32
 BF16 = jnp.bfloat16
 
@@ -395,10 +397,578 @@
       scaled, projected, squares, value_first, gate_first, value_second, gate_second)
 
 
+EXTRA = ()
+RELAY_X = (0, 1)
+RELAY_Y = (2, 3)
+
+
+def exchange_block(
+    mixer, value_cot, gate_cot, value_weight, gate_weight, value_basis, gate_basis,
+    value_first, gate_first, value_second, gate_second,
+    gathered, scaled, proj, squares_out, basis, weight, moments,
+    x_buf, cot_buf, gram, acc, first_in, second_out, second_in, part, part_in, sq_buf,
+    x_sem, c_sem, b_sem, w_sem, m_sem,
+    z_send, z_recv, x_send, x_recv, y_send, y_recv, rx_send, rx_recv, ry_send, ry_recv,
+    s1_send, s1_recv, s2_send, s2_recv, s3_send, s3_recv, a_send, a_recv,
+    g_send, g_recv, p_send, p_recv, q_send, q_recv,
+):
+    f, r, t = lax.axis_index("fs"), lax.axis_index("rep"), lax.axis_index("tp")
+    n_fs = 4
+    cots = (value_cot, gate_cot)
+    weights = (value_weight, gate_weight)
+    bases = (value_basis, gate_basis)
+    tokens = mixer.shape[0]
+    chunk = tokens // CHUNKS
+    rows = value_weight.shape[0]
+    share = rows // 4
+    piece_rows = share // 2
+    low = moments.shape[1]
+    width = acc.shape[3]
+    ends = jnp.logical_or(f == 0, f == n_fs - 1)
+    inner = jnp.logical_not(ends)
+    turn = 1 - 2 * (f // 2)
+    ahead = f + turn
+    behind = jnp.clip(f - turn, 0, n_fs - 1)
+    x_at, y_at = lax.rem(r, 2), r // 2
+    x_peer, y_peer = r + 1 - 2 * x_at, r + 2 - 4 * y_at
+    across = 3 - r
+    half_at, part_at = (x_at, y_at), (y_at, x_at)
+    half_peer, part_peer = (x_peer, y_peer), (y_peer, x_peer)
+    mine = [2 * half_at[k] + part_at[k] for k in range(2)]
+
+    def fs_at(d):
+        return lax.rem(f + d, n_fs)
+
+    def send(src, dst, s, v, **where):
+        return pltpu.make_async_remote_copy(
+            src_ref=src, dst_ref=dst, send_sem=s, recv_sem=v,
+            device_id=where, device_id_type=pl.DeviceIdType.MESH,
+        )
+
+    def span(start, size):
+        return pl.ds(pl.multiple_of(start, size), size)
+
+    def piece(plane, quarter, c):
+        return gathered.at[c % 2, span(plane * rows + quarter * share + (c // 2) * piece_rows, piece_rows)]
+
+    z_pieces = [(r, c) for c in range(4)] + [(across, c) for c in EXTRA]
+    count = len(z_pieces)
+    order = (r, across, x_peer, y_peer)
+
+    def w_load(o, k):
+        where = span(order[o] * share, share)
+        return pltpu.make_async_copy(weights[k].at[where], weight.at[k, where], w_sem.at[o, k])
+
+    def b_load(k):
+        return pltpu.make_async_copy(bases[k], basis.at[k], b_sem.at[k])
+
+    def x_load(c):
+        return pltpu.make_async_copy(mixer.at[span(c * chunk, chunk)], x_buf.at[c], x_sem.at[c])
+
+    def c_load(k, c):
+        return pltpu.make_async_copy(cots[k].at[span(c * chunk, chunk)], cot_buf.at[k, c], c_sem.at[k, c])
+
+    m_loads = [
+        pltpu.make_async_copy(ref, moments.at[i], m_sem.at[i])
+        for i, ref in enumerate((value_first, gate_first, value_second, gate_second))
+    ]
+    for k in range(2):
+        w_load(0, k).start()
+    if EXTRA:
+        for k in range(2):
+            w_load(1, k).start()
+    b_load(0).start()
+    for c in range(CHUNKS):
+        x_load(c).start()
+        c_load(0, c).start()
+    b_load(1).start()
+    for c in range(CHUNKS):
+        c_load(1, c).start()
+    for copy in m_loads:
+        copy.start()
+    for o in range(2 if EXTRA else 1, 4):
+        for k in range(2):
+            w_load(o, k).start()
+
+    barrier = pltpu.get_barrier_semaphore()
+    for d in range(1, n_fs):
+        pl.semaphore_signal(barrier, inc=1, device_id={"fs": fs_at(d)}, device_id_type=pl.DeviceIdType.MESH)
+    for peer in (x_peer, y_peer):
+        pl.semaphore_signal(barrier, inc=1, device_id={"rep": peer}, device_id_type=pl.DeviceIdType.MESH)
+    pl.semaphore_signal(barrier, inc=1, device_id={"tp": 1 - t}, device_id_type=pl.DeviceIdType.MESH)
+
+    for o in range(2 if EXTRA else 1):
+        where = span(order[o] * share, share)
+        for k in range(2):
+            w_load(o, k).wait()
+            gathered[k, span(f * rows + order[o] * share, share)] = weight[k, where].astype(BF16)
+    pl.semaphore_wait(barrier, n_fs + 2)
+
+    def plane_of(slot):
+        return lax.rem(f + turn * slot + n_fs, n_fs)
+
+    landing = jnp.where(ends, 2, 0)
+
+    def own_ahead(i):
+        quarter, c = z_pieces[i]
+        ref = piece(f, quarter, c)
+        return send(ref, ref, z_send.at[0, i], z_recv.at[landing, i], fs=ahead)
+
+    def own_behind(i):
+        quarter, c = z_pieces[i]
+        ref = piece(f, quarter, c)
+        return send(ref, ref, z_send.at[1, i], z_recv.at[0, i], fs=behind)
+
+    def pass_along(slot, i):
+        quarter, c = z_pieces[i]
+        ref = piece(plane_of(slot), quarter, c)
+        if slot == 3:
+            return send(ref, ref, z_send.at[4, i], z_recv.at[1, i], fs=ahead)
+        return send(ref, ref, z_send.at[1 + slot, i], z_recv.at[slot, i], fs=behind)
+
+    def arrival(slot, i):
+        quarter, c = z_pieces[i]
+        ref = piece(plane_of(slot), quarter, c)
+        return send(ref, ref, z_send.at[0, i], z_recv.at[slot - 1, i], fs=ahead)
+
+    for i in range(count):
+        own_ahead(i).start()
+
+        @pl.when(inner)
+        def _():
+            own_behind(i).start()
+
+    def to_x(slot, c):
+        ref = piece(plane_of(slot), r, c)
+        return send(ref, ref, x_send.at[slot - 1, c], x_recv.at[slot - 1, c], rep=x_peer)
+
+    def to_y(slot, c):
+        ref = piece(plane_of(slot), r, c)
+        return send(ref, ref, y_send.at[slot - 1, c], y_recv.at[slot - 1, c], rep=y_peer)
+
+    def relay_x(slot, c):
+        ref = piece(plane_of(slot), y_peer, c)
+        return send(ref, ref, rx_send.at[slot - 1, c], rx_recv.at[slot - 1, c], rep=x_peer)
+
+    def relay_y(slot, c):
+        ref = piece(plane_of(slot), x_peer, c)
+        return send(ref, ref, ry_send.at[slot - 1, c], ry_recv.at[slot - 1, c], rep=y_peer)
+
+    def spread(slot, i):
+        if i < 4:
+            to_x(slot, i).start()
+            to_y(slot, i).start()
+
+    def arrive_first(i):
+        arrival(1, i).wait_recv()
+
+        @pl.when(inner)
+        def _():
+            pass_along(1, i).start()
+
+        spread(1, i)
+
+    def arrive_inner(i):
+        @pl.when(inner)
+        def _():
+            arrival(3, i).wait_recv()
+            pass_along(3, i).start()
+
+    def arrive_second(i):
+        arrival(2, i).wait_recv()
+
+        @pl.when(inner)
+        def _():
+            pass_along(2, i).start()
+
+        spread(2, i)
+
+    def arrive_third(i):
+        @pl.when(ends)
+        def _():
+            arrival(3, i).wait_recv()
+
+        spread(3, i)
+
+    def relay(slot, c):
+        if c in RELAY_X:
+            to_y(slot, c).wait_recv()
+            relay_x(slot, c).start()
+        if c in RELAY_Y:
+            to_x(slot, c).wait_recv()
+            relay_y(slot, c).start()
+
+    def s1(k):
+        other = acc.at[k, pl.ds(2 * (1 - half_at[k]), 2)]
+        return send(other, first_in.at[k], s1_send.at[k], s1_recv.at[k], rep=half_peer[k])
+
+    def s2(k):
+        return send(second_out.at[k], second_in.at[k], s2_send.at[k], s2_recv.at[k], rep=part_peer[k])
+
+    def s3(k, d):
+        return send(
+            part.at[k, span(fs_at(d) * low, low)], part_in.at[k, d - 1],
+            s3_send.at[k, d - 1], s3_recv.at[k, d - 1], fs=fs_at(d),
+        )
+
+    def halve(k):
+        s1(k).wait_recv()
+        other = 1 - part_at[k]
+        second_out[k] = acc[k, 2 * half_at[k] + other] + first_in[k, other]
+        s2(k).start()
+        part[k] = acc[k, mine[k]] + first_in[k, part_at[k]]
+
+    def quarter(k):
+        s2(k).wait_recv()
+        part[k] += second_in[k]
+        for d in range(1, n_fs):
+            s3(k, d).start()
+
+    def a4(k, d):
+        ref = scaled.at[k, mine[k], span(f * low, low)]
+        return send(ref, ref, a_send.at[k, d - 1], a_recv.at[k, d - 1], fs=fs_at(d))
+
+    def grow(buf, ss, vs, k, stage):
+        if stage == 0:
+            ref = buf.at[k, mine[k]]
+            return send(ref, ref, ss.at[k, 0], vs.at[k, 0], rep=part_peer[k])
+        if stage == 1:
+            ref = buf.at[k, mine[k]]
+            return send(ref, ref, ss.at[k, 1], vs.at[k, 1], rep=half_peer[k])
+        ref = buf.at[k, 2 * half_at[k] + 1 - part_at[k]]
+        return send(ref, ref, ss.at[k, 2], vs.at[k, 2], rep=half_peer[k])
+
+    def g4(k, stage):
+        return grow(scaled, g_send, g_recv, k, stage)
+
+    def p4(k, stage):
+        return grow(proj, p_send, p_recv, k, stage)
+
+    def update(k):
+        if k == 0:
+            for copy in m_loads:
+                copy.wait()
+        for d in range(1, n_fs):
+            s3(k, d).wait_recv()
+        small = part[k, span(f * low, low)]
+        for d in range(1, n_fs):
+            small += part_in[k, d - 1]
+        proj[k, mine[k]] = small
+        cols = span(mine[k] * width, width)
+        first_new = 0.9 * moments[k, :, cols] + 0.1 * small
+        second_new = 0.95 * moments[2 + k, :, cols] + 0.05 * small * small
+        scaled[k, mine[k], span(f * low, low)] = (first_new * lax.rsqrt(second_new)).astype(BF16)
+        for d in range(1, n_fs):
+            a4(k, d).start()
+
+    def collect(k):
+        for d in range(1, n_fs):
+            a4(k, d).wait_recv()
+        g4(k, 0).start()
+        g4(k, 1).start()
+        p4(k, 0).start()
+        p4(k, 1).start()
+
+    def collect_second(k):
+        g4(k, 0).wait_recv()
+        g4(k, 2).start()
+        p4(k, 0).wait_recv()
+        p4(k, 2).start()
+
+    def measure(k):
+        for stage in (1, 2):
+            g4(k, stage).wait_recv()
+        squares = 0.0
+        for n in range(4):
+            s = scaled[k, n]
+            squares += jnp.sum((dot(gram[k, 0], s) + dot(gram[k, 1], s)) * s.astype(F32))
+        sq_buf[0, k] = jnp.full(sq_buf.shape[2:], squares, F32)
+
+    def make_gram():
+        for k in range(2):
+            upper, lower = split(dot_first(basis[k], basis[k]))
+            gram[k, 0] = upper
+            gram[k, 1] = lower
+
+    acc[...] = jnp.zeros_like(acc)
+    b_load(0).wait()
+
+    def one_step(i, carry):
+        k, c = i // CHUNKS, lax.rem(i, CHUNKS)
+
+        @pl.when(k == 0)
+        def _():
+            x_load(c).wait()
+            c_load(0, c).wait()
+
+        @pl.when(k == 1)
+        def _():
+            c_load(1, c).wait()
+
+        @pl.when(i == CHUNKS)
+        def _():
+            s1(0).start()
+            b_load(1).wait()
+
+        for at, job in ((CHUNKS + 1, 0), (CHUNKS + 3, 1)):
+            @pl.when(i == at)
+            def _():
+                arrive_first(job)
+                arrive_inner(job)
+
+        upper, lower = split(dot(x_buf[c], basis[k]))
+        for n in range(4):
+            cot = cot_buf[k, c, :, n * width : (n + 1) * width]
+            acc[k, n] += dot_first(upper, cot) + dot_first(lower, cot)
+        return carry
+
+    lax.fori_loop(0, 2 * CHUNKS, one_step, 0)
+    s1(1).start()
+
+    plan = []
+
+    def at(time, job, *args):
+        plan.append((time, len(plan), job, args))
+
+    beat = 2.85
+    for i in range(count):
+        if i > 1:
+            at(5 + beat * (i + 1), arrive_first, i)
+            at(5.1 + beat * (i + 1), arrive_inner, i)
+        at(8 + beat * (count + i + 1), arrive_second, i)
+        at(14 + beat * (2 * count + i + 1), arrive_third, i)
+    for c in range(4):
+        at(14 + beat * (c + 1), relay, 1, c)
+        at(17 + beat * (count + c + 1), relay, 2, c)
+        at(23 + beat * (2 * count + c + 1), relay, 3, c)
+    at(13, make_gram)
+    for k in range(2):
+        lag = 5 * k
+        at(17 + lag, halve, k)
+        at(23 + lag, quarter, k)
+        at(31 + lag, update, k)
+        at(38 + lag, collect, k)
+        at(44 + lag, collect_second, k)
+        at(52 + lag, measure, k)
+    for _, _, job, args in sorted(plan, key=lambda entry: entry[:2]):
+        job(*args)
+
+    q4 = send(sq_buf.at[0], sq_buf.at[1], q_send, q_recv, tp=1 - t)
+    q4.start()
+    for k in range(2):
+        for stage in (1, 2):
+            p4(k, stage).wait_recv()
+    for slot in (1, 2, 3):
+        for c in range(4):
+            if c not in RELAY_X:
+                to_y(slot, c).wait_recv()
+            else:
+                relay_x(slot, c).wait_recv()
+                relay_x(slot, c).wait_send()
+            if c not in RELAY_Y:
+                to_x(slot, c).wait_recv()
+            else:
+                relay_y(slot, c).wait_recv()
+                relay_y(slot, c).wait_send()
+            to_x(slot, c).wait_send()
+            to_y(slot, c).wait_send()
+    for i in range(count):
+        own_ahead(i).wait_send()
+
+        @pl.when(inner)
+        def _():
+            own_behind(i).wait_send()
+            for slot in (1, 2, 3):
+                pass_along(slot, i).wait_send()
+    for k in range(2):
+        s1(k).wait_send()
+        s2(k).wait_send()
+        for d in range(1, n_fs):
+            s3(k, d).wait_send()
+            a4(k, d).wait_send()
+        for stage in range(3):
+            g4(k, stage).wait_send()
+            p4(k, stage).wait_send()
+    for o in range(2 if EXTRA else 1, 4):
+        for k in range(2):
+            w_load(o, k).wait()
+    q4.wait()
+    squares_out[...] = sq_buf[0] + sq_buf[1]
+
+
+def finish_block(
+    entries, gathered, scaled, proj, squares, basis, weight, moments,
+    value_new, gate_new, value_copy, gate_copy, value_step, gate_step,
+    value_first_new, gate_first_new, value_second_new, gate_second_new,
+    new_buf, step_buf, copy_buf, moment_buf, new_sem, step_sem, copy_sem, moment_sem,
+):
+    f = lax.axis_index("fs")
+    rows = weight.shape[1]
+    model = gathered.shape[1]
+    width = scaled.shape[3]
+    block = min(rows, 256)
+    own = rows // block
+    blocks = model // block
+    news, copies, steps = (value_new, gate_new), (value_copy, gate_copy), (value_step, gate_step)
+    factors = [lax.rsqrt(squares[k, :1, :1] / entries + 1e-06) for k in range(2)]
+
+    def span(start, size):
+        return pl.ds(pl.multiple_of(start, size), size)
+
+    def row_of(b):
+        return lax.rem(f * own + b, blocks) * block
+
+    def new_out(k, b):
+        return pltpu.make_async_copy(
+            new_buf.at[k, span(b * block, block)], news[k].at[span(b * block, block)], new_sem.at[k, b])
+
+    def step_store(k, b):
+        return pltpu.make_async_copy(
+            step_buf.at[k, span(b * block, block)], steps[k].at[span(b * block, block)], step_sem.at[k, b])
+
+    def copy_out(k, b):
+        where = span(row_of(b), block)
+        return pltpu.make_async_copy(copy_buf.at[k, where], copies[k].at[where], copy_sem.at[k, b])
+
+    def own_block(b, carry):
+        for k in range(2):
+            where = span(row_of(b), block)
+            local_rows = span(b * block, block)
+            for n in range(4):
+                cols = slice(n * width, (n + 1) * width)
+                direction = dot(basis[k, where], scaled[k, n]) * factors[k]
+                updated = weight[k, local_rows, cols] - learn_rate * direction
+                step_buf[k, local_rows, cols] = direction
+                new_buf[k, local_rows, cols] = updated
+                copy_buf[k, where, cols] = updated.astype(BF16)
+            step_store(k, b).start()
+            new_out(k, b).start()
+            copy_out(k, b).start()
+        return carry
+
+    lax.fori_loop(0, own, own_block, 0)
+    outs = (value_first_new, gate_first_new, value_second_new, gate_second_new)
+    for k in range(2):
+        for n in range(4):
+            cols = slice(n * width, (n + 1) * width)
+            small = proj[k, n]
+            moment_buf[k, :, cols] = 0.9 * moments[k, :, cols] + 0.1 * small
+            moment_buf[2 + k, :, cols] = 0.95 * moments[2 + k, :, cols] + 0.05 * small * small
+    moment_outs = [pltpu.make_async_copy(moment_buf.at[i], outs[i], moment_sem.at[i]) for i in range(4)]
+    for copy in moment_outs:
+        copy.start()
+
+    def other_block(b, carry):
+        for k in range(2):
+            where = span(row_of(b), block)
+            for n in range(4):
+                cols = slice(n * width, (n + 1) * width)
+                direction = dot(basis[k, where], scaled[k, n]) * (learn_rate * factors[k])
+                copy_buf[k, where, cols] = (gathered[k, where, cols].astype(F32) - direction).astype(BF16)
+            copy_out(k, b).start()
+        return carry
+
+    lax.fori_loop(own, blocks, other_block, 0)
+
+    def drain_own(b, carry):
+        for k in range(2):
+            step_store(k, b).wait()
+            new_out(k, b).wait()
+        return carry
+
+    def drain(b, carry):
+        for k in range(2):
+            copy_out(k, b).wait()
+        return carry
+
+    lax.fori_loop(0, own, drain_own, 0)
+    lax.fori_loop(0, blocks, drain, 0)
+    for copy in moment_outs:
+        copy.wait()
+
+
+def local_block(*args):
+    (mixer, value_cot, gate_cot, value_weight, gate_weight, value_basis, gate_basis,
+     value_first, gate_first, value_second, gate_second) = args
+    n_fs = 4
+    tokens, model = mixer.shape
+    half = value_cot.shape[1]
+    rows = value_weight.shape[0]
+    rank = value_basis.shape[1]
+    low = value_first.shape[0]
+    width = half // 4
+    chunk = tokens // CHUNKS
+    count = 4 + len(EXTRA)
+    hbm = pl.BlockSpec(memory_space=pltpu.HBM)
+    vmem = pl.BlockSpec(memory_space=pltpu.VMEM)
+    dma = pltpu.SemaphoreType.DMA
+    scratch = [
+        pltpu.VMEM((CHUNKS, chunk, model), BF16),
+        pltpu.VMEM((2, CHUNKS, chunk, half), BF16),
+        pltpu.VMEM((2, 2, rank, rank), BF16),
+        pltpu.VMEM((2, 4, rank, width), F32),
+        pltpu.VMEM((2, 2, rank, width), F32),
+        pltpu.VMEM((2, rank, width), F32),
+        pltpu.VMEM((2, rank, width), F32),
+        pltpu.VMEM((2, rank, width), F32),
+        pltpu.VMEM((2, n_fs - 1, low, width), F32),
+        pltpu.VMEM((2, 2, 8, 128), F32),
+        dma((CHUNKS,)), dma((2, CHUNKS)), dma((2,)), dma((4, 2)), dma((4,)),
+        dma((5, count)), dma((3, count)),
+    ]
+    scratch += [dma((3, 4)) for _ in range(8)]
+    scratch += [dma((2,)) for _ in range(4)]
+    scratch += [dma((2, 3)) for _ in range(8)]
+    scratch += [dma(()), dma(())]
+    outs = pl.pallas_call(
+        exchange_block,
+        out_shape=(
+            pltpu.VMEM((2, model, half), BF16),
+            pltpu.VMEM((2, 4, rank, width), BF16),
+            pltpu.VMEM((2, 4, low, width), F32),
+            pltpu.VMEM((2, 8, 128), F32),
+            pltpu.VMEM((2, model, rank), BF16),
+            pltpu.VMEM((2, rows, half), F32),
+            pltpu.VMEM((4, low, half), F32),
+        ),
+        in_specs=[hbm] * 11,
+        out_specs=(vmem,) * 7,
+        scratch_shapes=scratch,
+        compiler_params=pltpu.CompilerParams(
+            collective_id=0, has_side_effects=True, vmem_limit_bytes=VMEM_FIRST
+        ),
+        name="exchange_block",
+    )(*args)
+    outs = [pltpu.with_memory_space_constraint(out, pltpu.VMEM) for out in outs]
+    block = min(rows, 256)
+    return pl.pallas_call(
+        functools.partial(finish_block, float(model) * half * 2),
+        in_specs=[vmem] * 7,
+        out_specs=[hbm] * 10,
+        out_shape=[
+            jax.ShapeDtypeStruct((rows, half), F32),
+            jax.ShapeDtypeStruct((rows, half), F32),
+            jax.ShapeDtypeStruct((model, half), BF16),
+            jax.ShapeDtypeStruct((model, half), BF16),
+            jax.ShapeDtypeStruct((rows, half), F32),
+            jax.ShapeDtypeStruct((rows, half), F32),
+        ] + [jax.ShapeDtypeStruct((low, half), F32)] * 4,
+        scratch_shapes=[
+            pltpu.VMEM((2, rows, half), F32),
+            pltpu.VMEM((2, rows, half), F32),
+            pltpu.VMEM((2, model, half), BF16),
+            pltpu.VMEM((4, low, half), F32),
+            dma((2, rows // block)), dma((2, rows // block)), dma((2, model // block)), dma((4,)),
+        ],
+        compiler_params=pltpu.CompilerParams(vmem_limit_bytes=VMEM_SECOND),
+        name="finish_block",
+    )(*outs)
+
+
 def solution(mesh):
     sizes = tuple(mesh.shape[name] for name in ("fs", "rep", "tp"))
     return jax.shard_map(
-        lambda *args: tuple(local(sizes, *args)),
+        lambda *args: tuple(local_block(*args) if sizes == (4, 4, 2) else local(sizes, *args)),
         mesh=mesh,
         in_specs=(
             P(("fs", "rep"), None),

time: 138 us -> 116 us (0.84)
  Pallas kernels: 129 us -> 115 us
  local copies, waits for them, and re-layouts: 7.22 us -> 0 us
    pallas_call x2, Pallas kernels: 129 us -> 115 us  [the longest x1 109 us: local_block(): pl.pallas_call(exchange_block, out_shape=(pltpu.VMEM((2, model, half), BF...]
    unnamed x24 -> x0, local copies, waits for them, and re-layouts: 7.22 us -> none
where the time goes in v1:
time: 116 us
  Pallas kernels  115 us (99%)
    pallas_call x1, Pallas kernels, local_block(): pl.pallas_call(exchange_block, out_shape=(pltpu.VMEM((2, model, half), BF...  109 us
    pallas_call x1, Pallas kernels, local_block(): pl.pallas_call(functools.partial(finish_block, float(model) * half * 2),...  6.75 us

profile of v1, /device:TPU:0, one launch (start us, length us, event | category | flops | bytes accessed | tf_op | source)
XLA Modules:
  0.0 116.0 jit_solution(1217846807473598345)
XLA Ops:
  0.6 108.6 %exchange_block.1 = (bf16[2,2048,1024]{2,1,0:T(8,128)(2,1)S(1)}, bf16[2,4,256,256]{3,2,1,0:T(8,128)(2,1)S(1)}, f32[2,4,64,256]{3,2,1,0:T(8,128)S(1)}, f32[2,8,12...) custom-call(bf16[2048,2048]{1,0:T(8,128)(2,1)} %mixer.1, ...), custom_call_target="tpu_custom_call" | custom-call | tf_op jit(solution)/shard_map/exchange_block/pallas_call | solution.py:923
  109.3 6.8 %finish_block.1 = (f32[512,1024]{1,0:T(8,128)}, f32[512,1024]{1,0:T(8,128)}, bf16[2048,1024]{1,0:T(8,128)(2,1)}, bf16[2048,1024]{1,0:T(8,128)(2,1)}, f32[512,102...) custom-call(bf16[2,2048,1024]{2,1,0:T(8,128)(2,1)S(1)} %get-tuple-el, ...), custom_call_target="tpu_custom_call" | custom-call | tf_op jit(solution)/shard_map/finish_block/pallas_call | solution.py:944

commit v2 on v1

--- a/solution.py
+++ b/solution.py
@@ -397,9 +397,22 @@
       scaled, projected, squares, value_first, gate_first, value_second, gate_second)
 
 
-EXTRA = ()
-RELAY_X = (0, 1)
-RELAY_Y = (2, 3)
+EXTRA = (0, 1)
+RELAY_X = (2,)
+RELAY_Y = (3,)
+EARLY = (
+    (2, "relay", 2, 0), (2, "first", 0), (4, "begin", 0), (4, "relay", 1, 0), (4, "first", 1),
+    (6, "first", 2),
+)
+LATE = (
+    ("relay", 3, 1), ("inner", 0), ("begin", 1), ("inner", 2), ("inner", 3), ("halve", 0), ("first", 3),
+    ("second", 2), ("halve", 1), ("inner", 1), ("third", 2), ("second", 3), ("gram",), ("relay", 1, 2),
+    ("relay", 1, 3), ("quarter", 0), ("relay", 3, 0), ("second", 0), ("second", 1), ("relay", 1, 1),
+    ("quarter", 1), ("third", 0), ("update", 0), ("inner", 4), ("inner", 5), ("update", 1), ("third", 1),
+    ("collect", 0), ("first", 4), ("third", 3), ("collect", 1), ("second", 4), ("again", 0), ("relay", 3, 3),
+    ("relay", 3, 2), ("relay", 2, 2), ("again", 1), ("first", 5), ("relay", 2, 3), ("relay", 2, 1),
+    ("second", 5), ("measure", 0), ("third", 4), ("measure", 1), ("third", 5),
+)
 
 
 def exchange_block(
@@ -653,7 +666,7 @@
         small = part[k, span(f * low, low)]
         for d in range(1, n_fs):
             small += part_in[k, d - 1]
-        proj[k, mine[k]] = small
+        proj[k, mine[k]] = small.astype(BF16)
         cols = span(mine[k] * width, width)
         first_new = 0.9 * moments[k, :, cols] + 0.1 * small
         second_new = 0.95 * moments[2 + k, :, cols] + 0.05 * small * small
@@ -690,6 +703,12 @@
             gram[k, 0] = upper
             gram[k, 1] = lower
 
+    jobs = {
+        "begin": lambda k: s1(k).start(), "first": arrive_first, "inner": arrive_inner,
+        "second": arrive_second, "third": arrive_third, "relay": relay, "halve": halve,
+        "quarter": quarter, "update": update, "collect": collect, "again": collect_second,
+        "measure": measure, "gram": make_gram,
+    }
     acc[...] = jnp.zeros_like(acc)
     b_load(0).wait()
 
@@ -707,51 +726,26 @@
 
         @pl.when(i == CHUNKS)
         def _():
-            s1(0).start()
             b_load(1).wait()
 
-        for at, job in ((CHUNKS + 1, 0), (CHUNKS + 3, 1)):
-            @pl.when(i == at)
+        for step in sorted({entry[0] for entry in EARLY}):
+            @pl.when(i == step)
             def _():
-                arrive_first(job)
-                arrive_inner(job)
-
-        upper, lower = split(dot(x_buf[c], basis[k]))
+                for entry in EARLY:
+                    if entry[0] == step:
+                        jobs[entry[1]](*entry[2:])
+
+        upper, lower = split(
+            lax.dot_general(basis[k], x_buf[c], (((0,), (1,)), ((), ())), preferred_element_type=F32)
+        )
         for n in range(4):
             cot = cot_buf[k, c, :, n * width : (n + 1) * width]
-            acc[k, n] += dot_first(upper, cot) + dot_first(lower, cot)
+            acc[k, n] += dot(upper, cot) + dot(lower, cot)
         return carry
 
     lax.fori_loop(0, 2 * CHUNKS, one_step, 0)
-    s1(1).start()
-
-    plan = []
-
-    def at(time, job, *args):
-        plan.append((time, len(plan), job, args))
-
-    beat = 2.85
-    for i in range(count):
-        if i > 1:
-            at(5 + beat * (i + 1), arrive_first, i)
-            at(5.1 + beat * (i + 1), arrive_inner, i)
-        at(8 + beat * (count + i + 1), arrive_second, i)
-        at(14 + beat * (2 * count + i + 1), arrive_third, i)
-    for c in range(4):
-        at(14 + beat * (c + 1), relay, 1, c)
-        at(17 + beat * (count + c + 1), relay, 2, c)
-        at(23 + beat * (2 * count + c + 1), relay, 3, c)
-    at(13, make_gram)
-    for k in range(2):
-        lag = 5 * k
-        at(17 + lag, halve, k)
-        at(23 + lag, quarter, k)
-        at(31 + lag, update, k)
-        at(38 + lag, collect, k)
-        at(44 + lag, collect_second, k)
-        at(52 + lag, measure, k)
-    for _, _, job, args in sorted(plan, key=lambda entry: entry[:2]):
-        job(*args)
+    for name, *where in LATE:
+        jobs[name](*where)
 
     q4 = send(sq_buf.at[0], sq_buf.at[1], q_send, q_recv, tp=1 - t)
     q4.start()
@@ -851,7 +845,7 @@
     for k in range(2):
         for n in range(4):
             cols = slice(n * width, (n + 1) * width)
-            small = proj[k, n]
+            small = proj[k, n].astype(F32)
             moment_buf[k, :, cols] = 0.9 * moments[k, :, cols] + 0.1 * small
             moment_buf[2 + k, :, cols] = 0.95 * moments[2 + k, :, cols] + 0.05 * small * small
     moment_outs = [pltpu.make_async_copy(moment_buf.at[i], outs[i], moment_sem.at[i]) for i in range(4)]
@@ -925,7 +919,7 @@
         out_shape=(
             pltpu.VMEM((2, model, half), BF16),
             pltpu.VMEM((2, 4, rank, width), BF16),
-            pltpu.VMEM((2, 4, low, width), F32),
+            pltpu.VMEM((2, 4, low, width), BF16),
             pltpu.VMEM((2, 8, 128), F32),
             pltpu.VMEM((2, model, rank), BF16),
             pltpu.VMEM((2, rows, half), F32),

time: 116 us -> 91.9 us (0.79)
  Pallas kernels: 115 us -> 91.1 us
    pallas_call x1, Pallas kernels: 109 us -> 84.3 us  [local_block(): pl.pallas_call(exchange_block, out_shape=(pltpu.VMEM((2, model, half), BF...]
where the time goes in v2:
time: 91.9 us; the launch traced here: 91.7 us
  Pallas kernels  91.1 us (99%)
    pallas_call x1, Pallas kernels, local_block(): pl.pallas_call(exchange_block, out_shape=(pltpu.VMEM((2, model, half), BF...  84.3 us
    pallas_call x1, Pallas kernels, local_block(): pl.pallas_call(functools.partial(finish_block, float(model) * half * 2),...  6.75 us

profile of v2, /device:TPU:0, one launch (start us, length us, event | category | flops | bytes accessed | tf_op | source)
XLA Modules:
  0.0 91.7 jit_solution(18220473538948624613)
XLA Ops:
  0.6 84.3 %exchange_block.1 = (bf16[2,2048,1024]{2,1,0:T(8,128)(2,1)S(1)}, bf16[2,4,256,256]{3,2,1,0:T(8,128)(2,1)S(1)}, bf16[2,4,64,256]{3,2,1,0:T(8,128)(2,1)S(1)}, f32[...) custom-call(bf16[2048,2048]{1,0:T(8,128)(2,1)} %mixer.1, ...), custom_call_target="tpu_custom_call" | custom-call | tf_op jit(solution)/shard_map/exchange_block/pallas_call | solution.py:917
  85.0 6.8 %finish_block.1 = (f32[512,1024]{1,0:T(8,128)}, f32[512,1024]{1,0:T(8,128)}, bf16[2048,1024]{1,0:T(8,128)(2,1)}, bf16[2048,1024]{1,0:T(8,128)(2,1)}, f32[512,102...) custom-call(bf16[2,2048,1024]{2,1,0:T(8,128)(2,1)S(1)} %get-tuple-el, ...), custom_call_target="tpu_custom_call" | custom-call | tf_op jit(solution)/shard_map/finish_block/pallas_call | solution.py:938

commit v3 on v2

--- a/solution.py
+++ b/solution.py
@@ -397,21 +397,27 @@
       scaled, projected, squares, value_first, gate_first, value_second, gate_second)
 
 
-EXTRA = (0, 1)
-RELAY_X = (2,)
-RELAY_Y = (3,)
+PIECES = 8
+EXTRA = (0, 1, 2, 3, 4)
+RELAY_X = ((5, 6), (5,), (5, 6))
+RELAY_Y = ((7,), (6, 7), (7,))
 EARLY = (
-    (2, "relay", 2, 0), (2, "first", 0), (4, "begin", 0), (4, "relay", 1, 0), (4, "first", 1),
-    (6, "first", 2),
+    (0, "open"), (2, "first", 0), (3, "first", 1), (4, "inner", 0), (4, "inner", 1), (4, "first", 2),
+    (6, "first", 3), (6, "first", 4), (6, "begin", 0, 0), (6, "inner", 4), (9, "begin", 0, 1),
+    (9, "first", 5), (9, "inner", 5), (9, "first", 6), (13, "begin", 1, 0), (13, "halve", 0),
+    (13, "inner", 9), (14, "relay", 1, 6), (14, "begin", 1, 1), (14, "inner", 2), (14, "inner", 6),
+    (14, "inner", 7), (15, "halve", 1), (15, "second", 2), (15, "inner", 8), (15, "inner", 12),
+    (15, "first", 7), (15, "inner", 3), (15, "second", 7), (15, "third", 2), (15, "second", 0),
+    (15, "quarter", 0), (15, "gram"), (15, "second", 5), (15, "third", 7), (15, "second", 6),
+    (15, "inner", 10), (15, "third", 0), (15, "second", 1),
 )
 LATE = (
-    ("relay", 3, 1), ("inner", 0), ("begin", 1), ("inner", 2), ("inner", 3), ("halve", 0), ("first", 3),
-    ("second", 2), ("halve", 1), ("inner", 1), ("third", 2), ("second", 3), ("gram",), ("relay", 1, 2),
-    ("relay", 1, 3), ("quarter", 0), ("relay", 3, 0), ("second", 0), ("second", 1), ("relay", 1, 1),
-    ("quarter", 1), ("third", 0), ("update", 0), ("inner", 4), ("inner", 5), ("update", 1), ("third", 1),
-    ("collect", 0), ("first", 4), ("third", 3), ("collect", 1), ("second", 4), ("again", 0), ("relay", 3, 3),
-    ("relay", 3, 2), ("relay", 2, 2), ("again", 1), ("first", 5), ("relay", 2, 3), ("relay", 2, 1),
-    ("second", 5), ("measure", 0), ("third", 4), ("measure", 1), ("third", 5),
+    ("relay", 1, 5), ("quarter", 1), ("second", 4), ("update", 0), ("first", 10), ("third", 5), ("third", 6),
+    ("relay", 3, 7), ("third", 1), ("first", 8), ("update", 1), ("second", 3), ("third", 4), ("collect", 0),
+    ("collect", 1), ("first", 9), ("inner", 11), ("first", 12), ("second", 10), ("relay", 3, 6), ("again", 0),
+    ("relay", 3, 5), ("third", 3), ("first", 11), ("relay", 2, 6), ("third", 10), ("second", 11),
+    ("second", 12), ("relay", 2, 5), ("again", 1), ("relay", 1, 7), ("third", 11), ("relay", 2, 7),
+    ("second", 9), ("second", 8), ("third", 9), ("third", 8), ("measure", 1), ("third", 12), ("measure", 0),
 )
 
 
@@ -419,7 +425,7 @@
     mixer, value_cot, gate_cot, value_weight, gate_weight, value_basis, gate_basis,
     value_first, gate_first, value_second, gate_second,
     gathered, scaled, proj, squares_out, basis, weight, moments,
-    x_buf, cot_buf, gram, acc, first_in, second_out, second_in, part, part_in, sq_buf,
+    x_buf, cot_buf, gram, turned, acc, first_in, second_out, second_in, part, part_in, sq_buf,
     x_sem, c_sem, b_sem, w_sem, m_sem,
     z_send, z_recv, x_send, x_recv, y_send, y_recv, rx_send, rx_recv, ry_send, ry_recv,
     s1_send, s1_recv, s2_send, s2_recv, s3_send, s3_recv, a_send, a_recv,
@@ -434,7 +440,7 @@
     chunk = tokens // CHUNKS
     rows = value_weight.shape[0]
     share = rows // 4
-    piece_rows = share // 2
+    piece_rows = 2 * share // PIECES
     low = moments.shape[1]
     width = acc.shape[3]
     ends = jnp.logical_or(f == 0, f == n_fs - 1)
@@ -464,7 +470,7 @@
     def piece(plane, quarter, c):
         return gathered.at[c % 2, span(plane * rows + quarter * share + (c // 2) * piece_rows, piece_rows)]
 
-    z_pieces = [(r, c) for c in range(4)] + [(across, c) for c in EXTRA]
+    z_pieces = [(r, c) for c in range(PIECES)] + [(across, c) for c in EXTRA]
     count = len(z_pieces)
     order = (r, across, x_peer, y_peer)
 
@@ -478,25 +484,23 @@
     def x_load(c):
         return pltpu.make_async_copy(mixer.at[span(c * chunk, chunk)], x_buf.at[c], x_sem.at[c])
 
-    def c_load(k, c):
-        return pltpu.make_async_copy(cots[k].at[span(c * chunk, chunk)], cot_buf.at[k, c], c_sem.at[k, c])
+    def c_load(k):
+        return pltpu.make_async_copy(cots[k], cot_buf.at[k], c_sem.at[k])
 
     m_loads = [
         pltpu.make_async_copy(ref, moments.at[i], m_sem.at[i])
         for i, ref in enumerate((value_first, gate_first, value_second, gate_second))
     ]
-    for k in range(2):
-        w_load(0, k).start()
-    if EXTRA:
+    b_load(0).start()
+    x_load(0).start()
+    for o in range(2 if EXTRA else 1):
         for k in range(2):
-            w_load(1, k).start()
-    b_load(0).start()
-    for c in range(CHUNKS):
+            w_load(o, k).start()
+    for c in range(1, CHUNKS):
         x_load(c).start()
-        c_load(0, c).start()
+    c_load(0).start()
     b_load(1).start()
-    for c in range(CHUNKS):
-        c_load(1, c).start()
+    c_load(1).start()
     for copy in m_loads:
         copy.start()
     for o in range(2 if EXTRA else 1, 4):
@@ -510,13 +514,6 @@
         pl.semaphore_signal(barrier, inc=1, device_id={"rep": peer}, device_id_type=pl.DeviceIdType.MESH)
     pl.semaphore_signal(barrier, inc=1, device_id={"tp": 1 - t}, device_id_type=pl.DeviceIdType.MESH)
 
-    for o in range(2 if EXTRA else 1):
-        where = span(order[o] * share, share)
-        for k in range(2):
-            w_load(o, k).wait()
-            gathered[k, span(f * rows + order[o] * share, share)] = weight[k, where].astype(BF16)
-    pl.semaphore_wait(barrier, n_fs + 2)
-
     def plane_of(slot):
         return lax.rem(f + turn * slot + n_fs, n_fs)
 
@@ -544,12 +541,19 @@
         ref = piece(plane_of(slot), quarter, c)
         return send(ref, ref, z_send.at[0, i], z_recv.at[slot - 1, i], fs=ahead)
 
-    for i in range(count):
-        own_ahead(i).start()
-
-        @pl.when(inner)
-        def _():
-            own_behind(i).start()
+    def opening():
+        for o in range(2 if EXTRA else 1):
+            where = span(order[o] * share, share)
+            for k in range(2):
+                w_load(o, k).wait()
+                gathered[k, span(f * rows + order[o] * share, share)] = weight[k, where].astype(BF16)
+        pl.semaphore_wait(barrier, n_fs + 2)
+        for i in range(count):
+            own_ahead(i).start()
+
+            @pl.when(inner)
+            def _():
+                own_behind(i).start()
 
     def to_x(slot, c):
         ref = piece(plane_of(slot), r, c)
@@ -568,7 +572,7 @@
         return send(ref, ref, ry_send.at[slot - 1, c], ry_recv.at[slot - 1, c], rep=y_peer)
 
     def spread(slot, i):
-        if i < 4:
+        if i < PIECES:
             to_x(slot, i).start()
             to_y(slot, i).start()
 
@@ -604,16 +608,16 @@
         spread(3, i)
 
     def relay(slot, c):
-        if c in RELAY_X:
+        if c in RELAY_X[slot - 1]:
             to_y(slot, c).wait_recv()
             relay_x(slot, c).start()
-        if c in RELAY_Y:
+        if c in RELAY_Y[slot - 1]:
             to_x(slot, c).wait_recv()
             relay_y(slot, c).start()
 
-    def s1(k):
-        other = acc.at[k, pl.ds(2 * (1 - half_at[k]), 2)]
-        return send(other, first_in.at[k], s1_send.at[k], s1_recv.at[k], rep=half_peer[k])
+    def s1(k, j):
+        other = acc.at[k, 2 * (1 - half_at[k]) + (part_at[k] if j else 1 - part_at[k])]
+        return send(other, first_in.at[k, j], s1_send.at[k, j], s1_recv.at[k, j], rep=half_peer[k])
 
     def s2(k):
         return send(second_out.at[k], second_in.at[k], s2_send.at[k], s2_recv.at[k], rep=part_peer[k])
@@ -625,15 +629,14 @@
         )
 
     def halve(k):
-        s1(k).wait_recv()
-        other = 1 - part_at[k]
-        second_out[k] = acc[k, 2 * half_at[k] + other] + first_in[k, other]
+        s1(k, 0).wait_recv()
+        second_out[k] = acc[k, 2 * half_at[k] + 1 - part_at[k]] + first_in[k, 0]
         s2(k).start()
-        part[k] = acc[k, mine[k]] + first_in[k, part_at[k]]
 
     def quarter(k):
+        s1(k, 1).wait_recv()
         s2(k).wait_recv()
-        part[k] += second_in[k]
+        part[k] = acc[k, mine[k]] + first_in[k, 1] + second_in[k]
         for d in range(1, n_fs):
             s3(k, d).start()
 
@@ -704,46 +707,56 @@
             gram[k, 1] = lower
 
     jobs = {
-        "begin": lambda k: s1(k).start(), "first": arrive_first, "inner": arrive_inner,
+        "open": opening, "begin": lambda k, j: s1(k, j).start(), "first": arrive_first, "inner": arrive_inner,
         "second": arrive_second, "third": arrive_third, "relay": relay, "halve": halve,
         "quarter": quarter, "update": update, "collect": collect, "again": collect_second,
         "measure": measure, "gram": make_gram,
     }
-    acc[...] = jnp.zeros_like(acc)
-    b_load(0).wait()
+    rank = basis.shape[2]
 
     def one_step(i, carry):
-        k, c = i // CHUNKS, lax.rem(i, CHUNKS)
-
-        @pl.when(k == 0)
-        def _():
-            x_load(c).wait()
-            c_load(0, c).wait()
-
-        @pl.when(k == 1)
-        def _():
-            c_load(1, c).wait()
-
-        @pl.when(i == CHUNKS)
-        def _():
-            b_load(1).wait()
-
-        for step in sorted({entry[0] for entry in EARLY}):
-            @pl.when(i == step)
+        k, at = i // (CHUNKS + 4), lax.rem(i, CHUNKS + 4)
+        for first in sorted({entry[0] for entry in EARLY}):
+            @pl.when(i == first)
             def _():
                 for entry in EARLY:
-                    if entry[0] == step:
+                    if entry[0] == first:
                         jobs[entry[1]](*entry[2:])
 
-        upper, lower = split(
-            lax.dot_general(basis[k], x_buf[c], (((0,), (1,)), ((), ())), preferred_element_type=F32)
-        )
-        for n in range(4):
-            cot = cot_buf[k, c, :, n * width : (n + 1) * width]
-            acc[k, n] += dot(upper, cot) + dot(lower, cot)
+        for role in range(2):
+            @pl.when(i == role * (CHUNKS + 4))
+            def _():
+                b_load(role).wait()
+
+            @pl.when(i == role * (CHUNKS + 4) + CHUNKS)
+            def _():
+                c_load(role).wait()
+
+        @pl.when(i < CHUNKS)
+        def _():
+            x_load(at).wait()
+
+        @pl.when(at < CHUNKS)
+        def _():
+            upper, lower = split(
+                lax.dot_general(basis[k], x_buf[at], (((0,), (1,)), ((), ())), preferred_element_type=F32)
+            )
+            turned[:rank, span(at * chunk, chunk)] = upper
+            turned[rank:, span(at * chunk, chunk)] = lower
+
+        @pl.when(at >= CHUNKS)
+        def _():
+            j = at - CHUNKS
+            half_on, part_on = jnp.where(k == 0, x_at, y_at), jnp.where(k == 0, y_at, x_at)
+            half_now = jnp.where(j < 2, 1 - half_on, half_on)
+            part_now = jnp.where(lax.rem(j, 2) == 0, 1 - part_on, part_on)
+            n = 2 * half_now + part_now
+            cot = cot_buf[k, :, span(n * width, width)]
+            acc[k, n] = dot(turned[:rank], cot) + dot(turned[rank:], cot)
+
         return carry
 
-    lax.fori_loop(0, 2 * CHUNKS, one_step, 0)
+    lax.fori_loop(0, 2 * (CHUNKS + 4), one_step, 0)
     for name, *where in LATE:
         jobs[name](*where)
 
@@ -753,13 +766,13 @@
         for stage in (1, 2):
             p4(k, stage).wait_recv()
     for slot in (1, 2, 3):
-        for c in range(4):
-            if c not in RELAY_X:
+        for c in range(PIECES):
+            if c not in RELAY_X[slot - 1]:
                 to_y(slot, c).wait_recv()
             else:
                 relay_x(slot, c).wait_recv()
                 relay_x(slot, c).wait_send()
-            if c not in RELAY_Y:
+            if c not in RELAY_Y[slot - 1]:
                 to_x(slot, c).wait_recv()
             else:
                 relay_y(slot, c).wait_recv()
@@ -775,7 +788,8 @@
             for slot in (1, 2, 3):
                 pass_along(slot, i).wait_send()
     for k in range(2):
-        s1(k).wait_send()
+        s1(k, 0).wait_send()
+        s1(k, 1).wait_send()
         s2(k).wait_send()
         for d in range(1, n_fs):
             s3(k, d).wait_send()
@@ -892,14 +906,15 @@
     low = value_first.shape[0]
     width = half // 4
     chunk = tokens // CHUNKS
-    count = 4 + len(EXTRA)
+    count = PIECES + len(EXTRA)
     hbm = pl.BlockSpec(memory_space=pltpu.HBM)
     vmem = pl.BlockSpec(memory_space=pltpu.VMEM)
     dma = pltpu.SemaphoreType.DMA
     scratch = [
         pltpu.VMEM((CHUNKS, chunk, model), BF16),
-        pltpu.VMEM((2, CHUNKS, chunk, half), BF16),
+        pltpu.VMEM((2, tokens, half), BF16),
         pltpu.VMEM((2, 2, rank, rank), BF16),
+        pltpu.VMEM((2 * rank, tokens), BF16),
         pltpu.VMEM((2, 4, rank, width), F32),
         pltpu.VMEM((2, 2, rank, width), F32),
         pltpu.VMEM((2, rank, width), F32),
@@ -907,11 +922,11 @@
         pltpu.VMEM((2, rank, width), F32),
         pltpu.VMEM((2, n_fs - 1, low, width), F32),
         pltpu.VMEM((2, 2, 8, 128), F32),
-        dma((CHUNKS,)), dma((2, CHUNKS)), dma((2,)), dma((4, 2)), dma((4,)),
+        dma((CHUNKS,)), dma((2,)), dma((2,)), dma((4, 2)), dma((4,)),
         dma((5, count)), dma((3, count)),
     ]
-    scratch += [dma((3, 4)) for _ in range(8)]
-    scratch += [dma((2,)) for _ in range(4)]
+    scratch += [dma((3, PIECES)) for _ in range(8)]
+    scratch += [dma((2, 2)), dma((2, 2)), dma((2,)), dma((2,))]
     scratch += [dma((2, 3)) for _ in range(8)]
     scratch += [dma(()), dma(())]
     outs = pl.pallas_call(

time: 91.9 us -> 89.5 us (0.974)
  Pallas kernels: 91.1 us -> 88.7 us
    pallas_call x1, Pallas kernels: 84.3 us -> 82 us  [local_block(): pl.pallas_call(exchange_block, out_shape=(pltpu.VMEM((2, model, half), BF...]
where the time goes in v3:
time: 89.5 us; the launch traced here: 89.4 us
  Pallas kernels  88.7 us (99%)
    pallas_call x1, Pallas kernels, local_block(): pl.pallas_call(exchange_block, out_shape=(pltpu.VMEM((2, model, half), BF...  82 us
    pallas_call x1, Pallas kernels, local_block(): pl.pallas_call(functools.partial(finish_block, float(model) * half * 2),...  6.75 us

profile of v3, /device:TPU:0, one launch (start us, length us, event | category | flops | bytes accessed | tf_op | source)
XLA Modules:
  0.0 89.4 jit_solution(3760178479007403657)
XLA Ops:
  0.6 82.0 %exchange_block.1 = (bf16[2,2048,1024]{2,1,0:T(8,128)(2,1)S(1)}, bf16[2,4,256,256]{3,2,1,0:T(8,128)(2,1)S(1)}, bf16[2,4,64,256]{3,2,1,0:T(8,128)(2,1)S(1)}, f32[...) custom-call(bf16[2048,2048]{1,0:T(8,128)(2,1)} %mixer.1, ...), custom_call_target="tpu_custom_call" | custom-call | tf_op jit(solution)/shard_map/exchange_block/pallas_call | solution.py:932
  82.6 6.8 %finish_block.1 = (f32[512,1024]{1,0:T(8,128)}, f32[512,1024]{1,0:T(8,128)}, bf16[2048,1024]{1,0:T(8,128)(2,1)}, bf16[2048,1024]{1,0:T(8,128)(2,1)}, f32[512,102...) custom-call(bf16[2,2048,1024]{2,1,0:T(8,128)(2,1)S(1)} %get-tuple-el, ...), custom_call_target="tpu_custom_call" | custom-call | tf_op jit(solution)/shard_map/finish_block/pallas_call | solution.py:953

commit v4 on v3

--- a/solution.py
+++ b/solution.py
@@ -402,22 +402,22 @@
 RELAY_X = ((5, 6), (5,), (5, 6))
 RELAY_Y = ((7,), (6, 7), (7,))
 EARLY = (
-    (0, "open"), (2, "first", 0), (3, "first", 1), (4, "inner", 0), (4, "inner", 1), (4, "first", 2),
-    (6, "first", 3), (6, "first", 4), (6, "begin", 0, 0), (6, "inner", 4), (9, "begin", 0, 1),
-    (9, "first", 5), (9, "inner", 5), (9, "first", 6), (13, "begin", 1, 0), (13, "halve", 0),
-    (13, "inner", 9), (14, "relay", 1, 6), (14, "begin", 1, 1), (14, "inner", 2), (14, "inner", 6),
-    (14, "inner", 7), (15, "halve", 1), (15, "second", 2), (15, "inner", 8), (15, "inner", 12),
-    (15, "first", 7), (15, "inner", 3), (15, "second", 7), (15, "third", 2), (15, "second", 0),
+    (0, "open"), (2, "first", 0), (3, "first", 1), (4, "inner", 1), (4, "first", 2), (6, "first", 3),
+    (6, "first", 4), (6, "inner", 4), (7, "begin", 0, 0), (9, "begin", 0, 1), (9, "first", 5),
+    (9, "inner", 5), (9, "first", 6), (13, "begin", 1, 0), (13, "halve", 0), (13, "inner", 9),
+    (14, "relay", 1, 6), (14, "begin", 1, 1), (14, "inner", 2), (14, "inner", 7), (15, "inner", 0),
+    (15, "halve", 1), (15, "second", 2), (15, "inner", 12), (15, "first", 7), (15, "inner", 3),
+    (15, "inner", 8), (15, "second", 7), (15, "inner", 6), (15, "third", 2), (15, "second", 0),
     (15, "quarter", 0), (15, "gram"), (15, "second", 5), (15, "third", 7), (15, "second", 6),
     (15, "inner", 10), (15, "third", 0), (15, "second", 1),
 )
 LATE = (
     ("relay", 1, 5), ("quarter", 1), ("second", 4), ("update", 0), ("first", 10), ("third", 5), ("third", 6),
     ("relay", 3, 7), ("third", 1), ("first", 8), ("update", 1), ("second", 3), ("third", 4), ("collect", 0),
-    ("collect", 1), ("first", 9), ("inner", 11), ("first", 12), ("second", 10), ("relay", 3, 6), ("again", 0),
-    ("relay", 3, 5), ("third", 3), ("first", 11), ("relay", 2, 6), ("third", 10), ("second", 11),
-    ("second", 12), ("relay", 2, 5), ("again", 1), ("relay", 1, 7), ("third", 11), ("relay", 2, 7),
-    ("second", 9), ("second", 8), ("third", 9), ("third", 8), ("measure", 1), ("third", 12), ("measure", 0),
+    ("collect", 1), ("first", 9), ("first", 12), ("inner", 11), ("second", 10), ("relay", 3, 6), ("again", 0),
+    ("first", 11), ("second", 9), ("relay", 2, 6), ("third", 3), ("relay", 3, 5), ("second", 11),
+    ("relay", 2, 5), ("again", 1), ("relay", 1, 7), ("third", 10), ("third", 11), ("second", 12),
+    ("relay", 2, 7), ("second", 8), ("third", 9), ("third", 8), ("measure", 1), ("third", 12), ("measure", 0),
 )
 
 
@@ -691,6 +691,9 @@
         p4(k, 0).wait_recv()
         p4(k, 2).start()
 
+    measured = []
+    q4 = send(sq_buf.at[0], sq_buf.at[1], q_send, q_recv, tp=1 - t)
+
     def measure(k):
         for stage in (1, 2):
             g4(k, stage).wait_recv()
@@ -699,6 +702,9 @@
             s = scaled[k, n]
             squares += jnp.sum((dot(gram[k, 0], s) + dot(gram[k, 1], s)) * s.astype(F32))
         sq_buf[0, k] = jnp.full(sq_buf.shape[2:], squares, F32)
+        measured.append(k)
+        if len(measured) == 2:
+            q4.start()
 
     def make_gram():
         for k in range(2):
@@ -760,8 +766,6 @@
     for name, *where in LATE:
         jobs[name](*where)
 
-    q4 = send(sq_buf.at[0], sq_buf.at[1], q_send, q_recv, tp=1 - t)
-    q4.start()
     for k in range(2):
         for stage in (1, 2):
             p4(k, stage).wait_recv()

time: 89.5 us -> 89.5 us (level)
  no operation moved by 1% of the time
where the time goes in v4:
time: 89.5 us; the launch traced here: 89.4 us
  Pallas kernels  88.7 us (99%)
    pallas_call x1, Pallas kernels, local_block(): pl.pallas_call(exchange_block, out_shape=(pltpu.VMEM((2, model, half), BF...  82 us
    pallas_call x1, Pallas kernels, local_block(): pl.pallas_call(functools.partial(finish_block, float(model) * half * 2),...  6.75 us

profile of v4, /device:TPU:0, one launch (start us, length us, event | category | flops | bytes accessed | tf_op | source)
XLA Modules:
  0.0 89.4 jit_solution(1685908321375204301)
XLA Ops:
  0.6 82.0 %exchange_block.1 = (bf16[2,2048,1024]{2,1,0:T(8,128)(2,1)S(1)}, bf16[2,4,256,256]{3,2,1,0:T(8,128)(2,1)S(1)}, bf16[2,4,64,256]{3,2,1,0:T(8,128)(2,1)S(1)}, f32[...) custom-call(bf16[2048,2048]{1,0:T(8,128)(2,1)} %mixer.1, ...), custom_call_target="tpu_custom_call" | custom-call | tf_op jit(solution)/shard_map/exchange_block/pallas_call | solution.py:936
  82.6 6.8 %finish_block.1 = (f32[512,1024]{1,0:T(8,128)}, f32[512,1024]{1,0:T(8,128)}, bf16[2048,1024]{1,0:T(8,128)(2,1)}, bf16[2048,1024]{1,0:T(8,128)(2,1)}, f32[512,102...) custom-call(bf16[2,2048,1024]{2,1,0:T(8,128)(2,1)S(1)} %get-tuple-el, ...), custom_call_target="tpu_custom_call" | custom-call | tf_op jit(solution)/shard_map/finish_block/pallas_call | solution.py:957
